TPU v7x, 32 devices: a whole 2x2x4 slice. The times are simulated.
32 devices in a mesh: grp: 2 (over y), sp: 4 (over z), tp: 4 (over x, core).
Axes of the slice: x: 2, y: 2, z: 4, core: 2. Of those that a mesh axis runs over, the one named last changes fastest.
Arguments:
- query_wide: bfloat16 [4096, 1024], P(('grp', 'sp'), 'tp'), parts along dimension 0, may hold values from -6 to 6
- key_wide: bfloat16 [4096, 1024], P(('grp', 'sp'), 'tp'), parts along dimension 0, may hold values from -6 to 6
- value_wide: bfloat16 [4096, 1024], P(('grp', 'sp'), 'tp'), parts along dimension 0, may hold values from -6 to 6
- decay_wide: float32 [4096, 8], P(('grp', 'sp'), 'tp'), parts along dimension 0, may hold values from -2 to 0, as said below
- query_narrow: bfloat16 [4096, 1024], P(('grp', 'sp'), 'tp'), parts along dimension 0, may hold values from -6 to 6
- key_narrow: bfloat16 [4096, 1024], P(('grp', 'sp'), 'tp'), parts along dimension 0, may hold values from -6 to 6
- value_narrow: bfloat16 [4096, 1024], P(('grp', 'sp'), 'tp'), parts along dimension 0, may hold values from -6 to 6
- decay_narrow: float32 [4096, 16], P(('grp', 'sp'), 'tp'), parts along dimension 0, may hold values from -2 to 0, as said below
- residual: bfloat16 [4096, 2048], P(('grp', 'sp', 'tp')), parts along dimension 0, may hold values from -6 to 6
- out_wide: bfloat16 [1024, 2048], P('tp'), may hold values from -0.125 to 0.125
- out_narrow: bfloat16 [1024, 2048], P('tp'), may hold values from -0.125 to 0.125
- norm_gain: float32 [2048], replicated, may hold values from 0.1 to 1.9
- routes: int32 [4096, 2], P(('grp', 'sp', 'tp')), parts along dimension 0, may hold values from 0 to 3, all different within a row; in each aligned block of 128 rows (0 to 127, 128 to 255, ...) at most 96 rows name the same one
- route_weights: float32 [4096, 2], P(('grp', 'sp', 'tp')), parts along dimension 0, may hold values from 0.1 to 1
- expert_gate: bfloat16 [4, 2048, 2048], P('sp', None, 'tp'), may hold values from -0.375 to 0.375
- expert_up: bfloat16 [4, 2048, 2048], P('sp', None, 'tp'), may hold values from -0.375 to 0.375
- expert_down: bfloat16 [4, 2048, 2048], P('sp', 'tp'), may hold values from -0.03125 to 0.03125
Outputs:
- layer_out: bfloat16 [4096, 2048], P(('grp', 'sp', 'tp')), parts along dimension 0
There are 2 independent parts, one for each index of `grp`. A program takes and returns all parts, laid end to end along the dimension named above; an argument that names none is the same for every part. Nothing has to cross between parts.
Inputs may be any that keep to these rules, and one draw needn't show every extreme that they name: `decay_wide`: every entry is negative. `decay_narrow`: every entry is negative. `routes`: each row names 2 different experts; on the rows of one device no expert is named more than 96 times, a bound that some block reaches.
All inputs are finite; a program needn't handle non-finite values.
Results may differ from a plain program's by a relative error of at most 0.018.
Values may be sent and summed in bfloat16 or wider, within the bound.
A program may use at most 128 MiB of HBM per device.

v0:
```python
import functools

import jax
import jax.numpy as jnp
from jax import lax
from jax.experimental import pallas as pl
from jax.experimental.pallas import tpu as pltpu
from jax.sharding import PartitionSpec as P

HEAD_WIDE = 128
HEAD_NARROW = 64
TOP_K = 2


norm_eps = 1e-05
clamp_limit = 7.0
swish_alpha = 1.702
rotary_base = 10000.0


def activate(gate_pre, up_pre):
    gate_clip = jnp.minimum(gate_pre, clamp_limit)
    up_clip = jnp.clip(up_pre, -clamp_limit, clamp_limit)
    return gate_clip * jax.nn.sigmoid(swish_alpha * gate_clip) * (up_clip + 1.0)


MESH = pl.DeviceIdType.MESH


def tail_kernel(
    experts,
    capacity,
    queries,
    queries_narrow,
    keys,
    keys_narrow,
    values,
    values_narrow,
    log_columns,
    log_rows,
    turns,
    out_wide,
    out_narrow,
    residual,
    gain,
    scatter,
    pick,
    weights,
    gate_hbm,
    up_hbm,
    down_hbm,
    output,
    gate,
    up,
    down,
    part,
    part_in,
    cross,
    cross_in,
    hidden_state,
    send,
    rows,
    result,
    result_in,
    half,
    half_in,
    summed,
    returned,
    mixed,
    inner,
    turned,
    local_state,
    local_total,
    states,
    totals,
    load_sem,
    s_send,
    s_recv,
    t_send,
    t_recv,
    a_send,
    a_recv,
    z_send,
    z_recv,
    x_send,
    x_recv,
    p_send,
    p_recv,
    c_send,
    c_recv,
    h_send,
    h_recv,
    r_send,
    r_recv,
):
    place = lax.axis_index("sp")
    mine = lax.axis_index("tp")
    core, side = mine % 2, mine // 2
    partner = side * 2 + (1 - core)
    across = (1 - side) * 2 + core
    model_width = residual.shape[1]

    def remote(src, dst, send_sem, recv_sem, **where):
        return pltpu.make_async_remote_copy(
            src_ref=src,
            dst_ref=dst,
            send_sem=send_sem,
            recv_sem=recv_sem,
            device_id=where,
            device_id_type=MESH,
        )

    def peer(step):
        return lax.rem(place + step, experts) if experts & (experts - 1) else place ^ step

    loads = [
        pltpu.make_async_copy(src, dst, load_sem.at[n])
        for n, (src, dst) in enumerate(((gate_hbm, gate), (up_hbm, up), (down_hbm, down)))
    ]
    for load in loads:
        load.start()

    barrier = pltpu.get_barrier_semaphore()
    pl.semaphore_signal(barrier, inc=1, device_id={"tp": partner}, device_id_type=MESH)
    pl.semaphore_signal(barrier, inc=1, device_id={"tp": across}, device_id_type=MESH)

    @pl.loop(1, experts)
    def _(step):
        pl.semaphore_signal(barrier, inc=1, device_id={"sp": peer(step)}, device_id_type=MESH)

    length = queries.shape[0]
    lane = lax.broadcasted_iota(jnp.int32, (1, 128), 1)
    first = lane < HEAD_NARROW
    rows_128 = lax.broadcasted_iota(jnp.int32, (128, 128), 0)
    lanes_128 = lax.broadcasted_iota(jnp.int32, (128, 128), 1)
    diagonal = (rows_128 < HEAD_NARROW) == (lanes_128 < HEAD_NARROW)
    flips = []
    for width in (HEAD_WIDE, HEAD_NARROW):
        half_width = width // 2
        upper = lanes_128 % width >= half_width
        origin = jnp.where(upper, lanes_128 - half_width, lanes_128 + half_width)
        flips.append(
            jnp.where(rows_128 == origin, jnp.where(upper, 1.0, -1.0), 0.0).astype(jnp.bfloat16)
        )

    def unit_of(wide_ref, narrow_ref, unit):
        ref = narrow_ref if unit >= 2 else wide_ref
        return ref[:, unit % 2 * 128 : unit % 2 * 128 + 128]

    def per_lane(unit, table):
        if unit < 2:
            return table(unit)
        return jnp.where(first, table(2 * unit - 2), table(2 * unit - 1))

    def heads_of(unit):
        if unit < 2:
            return ((unit, None),)
        return ((2 * unit - 2, first), (2 * unit - 1, ~first))

    def masked(value, keep):
        return value if keep is None else jnp.where(keep, value, jnp.zeros_like(value))

    def swapped(value):
        return pltpu.roll(value, HEAD_NARROW, 1)

    packed = []
    for unit in range(4):
        narrow = unit // 2
        cosine, sine_part = turns[narrow, 0], turns[narrow, 1]
        width = (HEAD_WIDE, HEAD_NARROW)[narrow]
        for n, refs in enumerate(((queries, queries_narrow), (keys, keys_narrow))):
            value = unit_of(*refs, unit)
            flipped = jnp.dot(value, flips[narrow], preferred_element_type=jnp.float32)
            value = value.astype(jnp.float32) * cosine + flipped * sine_part
            if n == 1:
                value = value * width ** (-0.5)
            turned[n, unit] = value.astype(jnp.bfloat16)
        gap = per_lane(
            unit,
            lambda head: log_columns[length - 1 : length, head : head + 1]
            - log_columns[:, head : head + 1],
        )
        weighted = (turned[1, unit].astype(jnp.float32) * jnp.exp(gap)).astype(jnp.bfloat16)
        state = lax.dot_general(
            weighted,
            unit_of(values, values_narrow, unit),
            (((0,), (0,)), ((), ())),
            preferred_element_type=jnp.float32,
        )
        last = log_columns[length - 1 : length, :]
        total_row = per_lane(
            unit, lambda head: jnp.broadcast_to(last[:, head : head + 1], (1, 128))
        )
        if unit == 3:
            state, total_row = swapped(state), swapped(total_row)
        packed.append(state)
        local_total[unit : unit + 1, :] = total_row
    for unit in range(4, 8):
        local_total[unit : unit + 1, :] = jnp.zeros((1, 128), jnp.float32)
    local_state[0] = packed[0].astype(jnp.bfloat16)
    local_state[1] = packed[1].astype(jnp.bfloat16)
    local_state[2] = jnp.where(diagonal, packed[2], packed[3]).astype(jnp.bfloat16)

    def send_state(source, target):
        return remote(
            local_state, states.at[source], s_send.at[target], s_recv.at[source], sp=target
        )

    def send_total(source, target):
        return remote(
            local_total, totals.at[source], t_send.at[target], t_recv.at[source], sp=target
        )

    pl.semaphore_wait(barrier, experts + 1)

    @pl.loop(place + 1, experts)
    def _(target):
        send_state(place, target).start()
        send_total(place, target).start()

    tile = min(length, 256)
    for unit in range(4):
        value = unit_of(values, values_narrow, unit)
        for start in range(0, length, tile):
            stop = start + tile
            steps = lax.broadcasted_iota(jnp.int32, (tile, stop), 0) + start
            causal = steps >= lax.broadcasted_iota(jnp.int32, (tile, stop), 1)
            total = jnp.zeros((tile, 128), jnp.float32)
            for head, keep in heads_of(unit):
                gaps = log_columns[start:stop, head : head + 1] - log_rows[head : head + 1, :stop]
                decay_grid = jnp.exp(jnp.where(causal, gaps, -1e30))
                scores = lax.dot_general(
                    masked(turned[0, unit, start:stop], keep),
                    turned[1, unit, :stop],
                    (((1,), (1,)), ((), ())),
                    preferred_element_type=jnp.float32,
                )
                total += jnp.dot(
                    (scores * decay_grid).astype(jnp.bfloat16),
                    masked(value[:stop], keep),
                    preferred_element_type=jnp.float32,
                )
            inner[unit, start:stop] = total

    def join(source, carried):
        send_state(source, source).wait_recv()
        send_total(source, source).wait_recv()
        fade = jnp.exp(totals[source])
        fade_narrow = jnp.where(diagonal, fade[2:3], fade[3:4])
        return (
            carried[0] * fade[0:1] + states[source, 0].astype(jnp.float32),
            carried[1] * fade[1:2] + states[source, 1].astype(jnp.float32),
            carried[2] * fade_narrow + states[source, 2].astype(jnp.float32),
        )

    nothing = jnp.zeros((128, 128), jnp.float32)
    carried = lax.fori_loop(0, place, join, (nothing, nothing, nothing))
    for unit in range(4):
        state = carried[min(unit, 2)]
        if unit == 2:
            state = jnp.where(diagonal, state, 0.0)
        if unit == 3:
            state = swapped(jnp.where(diagonal, 0.0, state))
        fade = jnp.exp(per_lane(unit, lambda head: log_columns[:, head : head + 1]))
        value = inner[unit] + fade * jnp.dot(
            turned[0, unit], state.astype(jnp.bfloat16), preferred_element_type=jnp.float32
        )

        def mean_of(value):
            if unit < 2:
                return jnp.mean(value, axis=-1, keepdims=True)
            low = jnp.sum(masked(value, first), axis=-1, keepdims=True)
            high = jnp.sum(masked(value, ~first), axis=-1, keepdims=True)
            return jnp.where(first, low, high) / HEAD_NARROW

        value = value - mean_of(value)
        spread = mean_of(value * value)
        mixed[:, unit * 128 : unit * 128 + 128] = (value * lax.rsqrt(spread + norm_eps)).astype(
            jnp.bfloat16
        )

    targets = (across // 2 * 2 + 1 - core, partner, across, mine)
    to_partner = [
        remote(part.at[n], part_in.at[n], a_send.at[n], a_recv.at[n], tp=partner)
        for n in range(2)
    ]
    to_across = remote(cross, cross_in, a_send.at[2], a_recv.at[2], tp=across)
    for n, target in enumerate(targets):
        rows_dev = residual.shape[0]
        picked = mixed[pl.ds(pl.multiple_of(target * rows_dev, rows_dev), rows_dev), :]
        part[n] = (
            jnp.dot(picked[:, :256], out_wide[...], preferred_element_type=jnp.float32)
            + jnp.dot(picked[:, 256:], out_narrow[...], preferred_element_type=jnp.float32)
        ).astype(jnp.bfloat16)
        if n < 2:
            to_partner[n].start()
        if n == 2:
            to_partner[0].wait_recv()
            cross[...] = (
                part[2].astype(jnp.float32) + part_in[0].astype(jnp.float32)
            ).astype(jnp.bfloat16)
            to_across.start()
    to_partner[1].wait_recv()
    hidden_state[...] = (
        residual[...].astype(jnp.float32)
        + part[3].astype(jnp.float32)
        + part_in[1].astype(jnp.float32)
    )
    to_across.wait_recv()
    total = hidden_state[...] + cross_in[...].astype(jnp.float32)
    hidden_state[...] = total
    scale_row = lax.rsqrt(jnp.mean(total * total, axis=-1, keepdims=True) + norm_eps)
    normed = (total * scale_row * gain[...]).astype(jnp.bfloat16)

    def slots(expert):
        return jnp.dot(scatter[expert], normed, preferred_element_type=jnp.float32).astype(
            jnp.bfloat16
        )

    def dispatch(expert):
        return remote(
            send.at[expert],
            rows.at[place, mine],
            z_send.at[expert],
            z_recv.at[place],
            sp=expert,
        )

    def arrived(source):
        return remote(
            send.at[source], rows.at[source, mine], z_send.at[source], z_recv.at[source], sp=source
        )

    def forward_across(source):
        return remote(
            rows.at[source, mine],
            rows.at[source, mine],
            x_send.at[source],
            x_recv.at[source],
            tp=across,
        )

    def forward_partner(source, n):
        block = (mine, across)[n]
        return remote(
            rows.at[source, block],
            rows.at[source, block],
            p_send.at[source, n],
            p_recv.at[source, n],
            tp=partner,
        )

    def swap(source):
        return remote(
            result.at[source, 1 - core],
            result_in.at[source],
            c_send.at[source],
            c_recv.at[source],
            tp=partner,
        )

    def swap_across(source):
        return remote(
            half.at[source], half_in.at[source], h_send.at[source], h_recv.at[source], tp=across
        )

    def give_back(source):
        return remote(
            summed.at[source],
            returned.at[place],
            r_send.at[source],
            r_recv.at[place],
            sp=source,
        )

    def came_back(expert):
        return remote(
            summed.at[expert],
            returned.at[expert],
            r_send.at[expert],
            r_recv.at[expert],
            sp=expert,
        )

    @pl.loop(1, experts)
    def _(step):
        expert = peer(step)
        send[expert] = slots(expert)
        dispatch(expert).start()

    rows[place, mine] = slots(place)
    forward_across(place).start()
    forward_partner(place, 0).start()

    for load in loads:
        load.wait()

    ff = gate.shape[1]
    ff_step = min(ff, 256)
    out_step = min(model_width, 512)

    def finish_across(source):
        swap_across(source).wait_recv()
        value = (
            result[source, core, side].astype(jnp.float32)
            + result_in[source, side].astype(jnp.float32)
            + half_in[source].astype(jnp.float32)
        ).astype(jnp.bfloat16)

        @pl.when(source == place)
        def _():
            returned[place] = value

        @pl.when(source != place)
        def _():
            summed[source] = value
            give_back(source).start()

    late = min(2, experts - 1)

    def halve(source):
        swap(source).wait_recv()
        half[source] = (
            result[source, core, 1 - side].astype(jnp.float32)
            + result_in[source, 1 - side].astype(jnp.float32)
        ).astype(jnp.bfloat16)
        swap_across(source).start()

    @pl.loop(0, experts)
    def _(step):
        source = peer(step)

        @pl.when(step + 1 < experts)
        def _():
            later = peer(step + 1)
            arrived(later).wait_recv()
            forward_across(later).start()
            forward_partner(later, 0).start()

        forward_across(source).wait_recv()
        forward_partner(source, 1).start()
        forward_partner(source, 0).wait_recv()
        forward_partner(source, 1).wait_recv()
        block = rows[source].reshape(4 * capacity, model_width)
        hidden = []
        for at in range(0, ff, ff_step):
            gate_pre = jnp.dot(
                block, gate[:, at : at + ff_step], preferred_element_type=jnp.float32
            )
            up_pre = jnp.dot(block, up[:, at : at + ff_step], preferred_element_type=jnp.float32)
            hidden.append(activate(gate_pre, up_pre).astype(jnp.bfloat16))
        hidden = jnp.concatenate(hidden, axis=1)
        for at in range(0, model_width, out_step):
            value = jnp.dot(
                hidden, down[:, at : at + out_step], preferred_element_type=jnp.float32
            ).astype(jnp.bfloat16)
            for n in range(4):
                result[source, n % 2, n // 2, :, at : at + out_step] = value[
                    n * capacity : (n + 1) * capacity
                ]
        swap(source).start()

        @pl.when(step >= late)
        def _():
            halve(source)

        @pl.when(step > late)
        def _():
            finish_across(peer(step - 1))

    waiting = experts - 1 if experts > late else None
    for step in range(late - 1, -1, -1):
        halve(peer(step))
        if waiting is not None:
            finish_across(peer(waiting))
        waiting = step
    finish_across(peer(waiting))

    @pl.loop(1, experts)
    def _(step):
        came_back(peer(step)).wait_recv()

    every = returned[...].reshape(experts * capacity, model_width)
    total = hidden_state[...]
    for k in range(TOP_K):
        total = total + weights[:, k : k + 1] * jnp.dot(
            pick[k], every, preferred_element_type=jnp.float32
        )
    output[...] = total.astype(output.dtype)

    @pl.loop(place + 1, experts)
    def _(target):
        send_state(place, target).wait_send()
        send_total(place, target).wait_send()

    to_partner[0].wait_send()
    to_partner[1].wait_send()
    to_across.wait_send()

    @pl.loop(0, experts)
    def _(step):
        source = peer(step)
        forward_across(source).wait_send()
        forward_partner(source, 0).wait_send()
        forward_partner(source, 1).wait_send()
        swap(source).wait_send()
        swap_across(source).wait_send()

        @pl.when(step >= 1)
        def _():
            dispatch(source).wait_send()
            give_back(source).wait_send()


def layer(mixer_inputs, outs, residual, norm_gain, routes, route_weights, gate, up, down):
    experts = lax.axis_size("sp")
    rows_dev, model_width = residual.shape
    length = mixer_inputs[0].shape[0]
    ff = gate.shape[1]
    limit = max(TOP_K, 3 * rows_dev * TOP_K // (2 * experts))
    capacity = -(-limit // 16) * 16
    names = jnp.arange(experts, dtype=jnp.int32)
    chosen = routes[:, :, None] == names[None, None, :]
    hits = jnp.any(chosen, axis=1)
    order = jnp.arange(rows_dev, dtype=jnp.int32)
    before = (order[:, None] > order[None, :]).astype(jnp.bfloat16)
    rank = jnp.dot(before, hits.astype(jnp.bfloat16), preferred_element_type=jnp.float32).astype(
        jnp.int32
    )
    slot = jnp.arange(capacity, dtype=jnp.int32)
    at_slot = rank[:, :, None] == slot[None, None, :]
    pick = (
        (chosen[:, :, :, None] & at_slot[:, None])
        .astype(jnp.bfloat16)
        .transpose(1, 0, 2, 3)
        .reshape(TOP_K, rows_dev, experts * capacity)
    )
    scatter = ((hits.T[:, None, :]) & (rank.T[:, None, :] == slot[None, :, None])).astype(
        jnp.bfloat16
    )
    bf16 = jnp.bfloat16
    block = (capacity, model_width)
    dma = pltpu.SemaphoreType.DMA
    vmem = pl.BlockSpec(memory_space=pltpu.VMEM)
    anywhere = pl.BlockSpec(memory_space=pl.ANY)
    return pl.pallas_call(
        functools.partial(tail_kernel, experts, capacity),
        out_shape=jax.ShapeDtypeStruct((rows_dev, model_width), bf16),
        in_specs=[vmem] * 16 + [anywhere] * 3,
        out_specs=vmem,
        scratch_shapes=[
            pltpu.VMEM((model_width, ff), bf16),
            pltpu.VMEM((model_width, ff), bf16),
            pltpu.VMEM((ff, model_width), bf16),
            pltpu.VMEM((4, rows_dev, model_width), bf16),
            pltpu.VMEM((2, rows_dev, model_width), bf16),
            pltpu.VMEM((rows_dev, model_width), bf16),
            pltpu.VMEM((rows_dev, model_width), bf16),
            pltpu.VMEM((rows_dev, model_width), jnp.float32),
            pltpu.VMEM((experts, *block), bf16),
            pltpu.VMEM((experts, 4, *block), bf16),
            pltpu.VMEM((experts, 2, 2, *block), bf16),
            pltpu.VMEM((experts, 2, *block), bf16),
            pltpu.VMEM((experts, *block), bf16),
            pltpu.VMEM((experts, *block), bf16),
            pltpu.VMEM((experts, *block), bf16),
            pltpu.VMEM((experts, *block), bf16),
            pltpu.VMEM((length, 512), bf16),
            pltpu.VMEM((4, length, 128), jnp.float32),
            pltpu.VMEM((2, 4, length, 128), bf16),
            pltpu.VMEM((3, 128, 128), bf16),
            pltpu.VMEM((8, 128), jnp.float32),
            pltpu.VMEM((experts, 3, 128, 128), bf16),
            pltpu.VMEM((experts, 8, 128), jnp.float32),
            dma((3,)),
            dma((experts,)),
            dma((experts,)),
            dma((experts,)),
            dma((experts,)),
            dma((3,)),
            dma((3,)),
            dma((experts,)),
            dma((experts,)),
            dma((experts,)),
            dma((experts,)),
            dma((experts, 2)),
            dma((experts, 2)),
            dma((experts,)),
            dma((experts,)),
            dma((experts,)),
            dma((experts,)),
            dma((experts,)),
            dma((experts,)),
        ],
        compiler_params=pltpu.CompilerParams(
            collective_id=1, has_side_effects=True, vmem_limit_bytes=60 * 1024 * 1024
        ),
    )(
        *mixer_inputs,
        *outs,
        residual,
        norm_gain.reshape(1, model_width),
        scatter,
        pick,
        route_weights,
        gate,
        up,
        down,
    )


def body(
    query_wide,
    key_wide,
    value_wide,
    decay_wide,
    query_narrow,
    key_narrow,
    value_narrow,
    decay_narrow,
    residual,
    out_wide,
    out_narrow,
    norm_gain,
    routes,
    route_weights,
    expert_gate,
    expert_up,
    expert_down,
):
    length = query_wide.shape[0]
    positions = (lax.axis_index("sp") * length + jnp.arange(length, dtype=jnp.int32)).astype(
        jnp.float32
    )
    tables = []
    for width in (HEAD_WIDE, HEAD_NARROW):
        half_width = width // 2
        inverse = rotary_base ** (-jnp.arange(half_width, dtype=jnp.float32) / half_width)
        angles = positions[:, None] * jnp.tile(inverse, 128 // half_width)[None, :]
        tables.append(jnp.stack([jnp.cos(angles), jnp.sin(angles)]))
    log_columns = jnp.cumsum(jnp.concatenate([decay_wide, decay_narrow], axis=1), axis=0)
    return layer(
        (
            query_wide,
            query_narrow,
            key_wide,
            key_narrow,
            value_wide,
            value_narrow,
            log_columns,
            log_columns.T,
            jnp.stack(tables),
        ),
        (out_wide, out_narrow),
        residual,
        norm_gain,
        routes,
        route_weights,
        expert_gate[0],
        expert_up[0],
        expert_down[0],
    )


def solution(mesh):
    placed = (
        P(("grp", "sp"), "tp"),
        P(("grp", "sp"), "tp"),
        P(("grp", "sp"), "tp"),
        P(("grp", "sp"), "tp"),
        P(("grp", "sp"), "tp"),
        P(("grp", "sp"), "tp"),
        P(("grp", "sp"), "tp"),
        P(("grp", "sp"), "tp"),
        P(("grp", "sp", "tp"), None),
        P("tp", None),
        P("tp", None),
        P(),
        P(("grp", "sp", "tp"), None),
        P(("grp", "sp", "tp"), None),
        P("sp", None, "tp"),
        P("sp", None, "tp"),
        P("sp", "tp", None),
    )
    return jax.shard_map(
        body, mesh=mesh, in_specs=placed, out_specs=P(("grp", "sp", "tp"), None), check_vma=False
    )
```

profile of v0, /device:TPU:0, one launch (start us, length us, event | category | flops | bytes accessed | tf_op | source)
XLA Modules:
  0.0 133.7 jit_solution(8187845232985492937)
XLA Ops:
  0.0 0.1 mul.58
  0.1 0.1 mul.55
  0.2 1.9 %multiply_cosine_fusion.1 = (f32[1,512,128]{2,1,0:T(8,128)S(1)}, f32[1,512,128]{2,1,0:T(8,128)S(1)}, f32[1,512,128]{2,1,0:T(8,128)S(1)}, f32[1,512,128]{2,1,0:T(8,128)S(1)}) fusion(f32[128]{0:T(128)S(1)} %mul.55, f32[512]{0:T(512)S(1)} %add_convert_fusion, f32[128]{0:T(128)S(1)} %mul.58), kind=kLoop, calls=%fused_computation.8 | loop fusion | flops 131072 | bytes 1051648 | tf_op jit(solution)/shard_map/cos | solution.py:640
  2.1 0.0 copy-start.1
  2.1 0.0 copy-start.2
  2.1 0.0 copy-start.4
  2.1 0.1 maximum_bitcast_fusion
  2.2 0.0 copy-start.3
  2.2 1.1 pad_maximum_fusion.turns
  3.3 0.0 copy-done.1
  3.3 0.0 copy-done.2
  3.3 1.8 %reduce-window.6 = f32[6,4,128]{2,1,0:T(4,128)S(1)} reduce-window(f32[6,4,128]{2,1,0:T(4,128)S(1)} %reshape.237, f32[]{:T(128)} %constant.6.clone.1), window={size=1x1x128 pad=0_0x0_0x127_0}, to_apply=%region_0.0 | reduce-window | flops 390144 | bytes 24580 | tf_op jit(solution)/shard_map/reduce-window
  5.2 0.1 slice.8
  5.2 0.1 copy.31
  5.4 0.1 copy.32
  5.5 0.1 add_bitcast_fusion
  5.6 0.0 copy-start
  5.6 0.9 copy.35.log_columns
  6.4 0.0 copy-done.4
  6.5 0.1 convolution_convert_fusion
  6.6 0.7 fusion.1.scatter
  7.3 0.1 eq.75
  7.4 0.1 bitcast_compare_fusion
  7.5 0.2 copy.33
  7.7 0.2 copy.34
  7.9 0.7 and_convert_fusion.pick
  8.6 0.0 copy-done.3
  8.7 0.7 copy.36.weights
  9.4 0.0 copy-done
  9.4 122.4 %shard_map.163 = bf16[128,2048]{1,0:T(8,128)(2,1)} custom-call(bf16[512,256]{1,0:T(8,128)(2,1)} %queries.1, bf16[512,256]{1,0:T(8,128)(2,1)} %queries_narrow.1, bf16[512,256]{1,0:T(8,128)(2,1)} %keys.1, bf16[512,256]{1,0:T(8,128)(2,1)} %keys_narrow.1, bf16[512,256]{1,0:T(8,128)(2,1)} %values.1, bf16[512,256]{1,0:T(8,128)(2,1)} %values_narrow.1, ...), custom_call_target="tpu_custom_call" | custom-call | tf_op jit(solution)/shard_map/pallas_call | solution.py:546
  131.8 1.9 %copy.43 = bf16[128,2048]{1,0:T(8,128)(2,1)} copy(bf16[128,2048]{1,0:T(8,128)(2,1)} %shard_map.163) | data formatting | bytes 1048576
  (14 shorter events, 0.2 us)
Async XLA Ops:
  2.1 1.2 copy-start.1
  2.1 1.2 copy-start.2
  2.1 4.3 %copy-start.4 = (s32[128,2]{0,1:T(2,128)S(1)}, s32[128,2]{0,1:T(2,128)}, u32[]{:S(2)}) copy-start(s32[128,2]{0,1:T(2,128)} %param.29) | copy-start | bytes 3076
  2.2 6.4 %copy-start.3 = (f32[128,2]{0,1:T(2,128)S(1)}, f32[128,2]{0,1:T(2,128)}, u32[]{:S(2)}) copy-start(f32[128,2]{0,1:T(2,128)} %param.30) | copy-start | bytes 3076
  5.6 3.8 %copy-start = (f32[1,6,4,128]{3,1,2,0:T(8,128)}, f32[1,6,4,128]{3,1,2,0:T(8,128)S(1)}, u32[]{:S(2)}) copy-start(f32[1,6,4,128]{3,1,2,0:T(8,128)S(1)} %copy.41) | copy-start | bytes 36868
where the time goes:
time: 134 us
  Pallas kernels  122 us (91%)
  other arithmetic  6.56 us (5%)
  local copies, waits for them, and re-layouts  4.46 us (3%)
    pallas_call x1, Pallas kernels, layer(): pl.pallas_call(functools.partial(tail_kernel, experts, capacity), out_sha...  122 us

commit v1 on v0

--- a/solution.py
+++ b/solution.py
@@ -2,6 +2,7 @@
 
 import jax
 import jax.numpy as jnp
+import numpy as np
 from jax import lax
 from jax.experimental import pallas as pl
 from jax.experimental.pallas import tpu as pltpu
@@ -30,29 +31,39 @@
 def tail_kernel(
     experts,
     capacity,
-    queries,
-    queries_narrow,
-    keys,
-    keys_narrow,
-    values,
-    values_narrow,
-    log_columns,
-    log_rows,
-    turns,
-    out_wide,
-    out_narrow,
-    residual,
-    gain,
-    scatter,
-    pick,
-    weights,
+    queries_hbm,
+    queries_narrow_hbm,
+    keys_hbm,
+    keys_narrow_hbm,
+    values_hbm,
+    values_narrow_hbm,
+    out_wide_hbm,
+    out_narrow_hbm,
+    residual_hbm,
     gate_hbm,
     up_hbm,
     down_hbm,
+    decay_wide,
+    decay_narrow,
+    coarse,
+    fine,
+    gain,
+    routes,
+    weights,
     output,
+    mixer_in,
+    outs_in,
+    residual,
     gate,
     up,
     down,
+    decays,
+    log_rows,
+    log_columns,
+    turns,
+    slot_rows,
+    slot_columns,
+    weight_columns,
     part,
     part_in,
     cross,
@@ -113,12 +124,30 @@
     def peer(step):
         return lax.rem(place + step, experts) if experts & (experts - 1) else place ^ step
 
-    loads = [
-        pltpu.make_async_copy(src, dst, load_sem.at[n])
-        for n, (src, dst) in enumerate(((gate_hbm, gate), (up_hbm, up), (down_hbm, down)))
+    sources = (
+        (keys_hbm, mixer_in.at[2]),
+        (keys_narrow_hbm, mixer_in.at[3]),
+        (values_hbm, mixer_in.at[4]),
+        (values_narrow_hbm, mixer_in.at[5]),
+        (queries_hbm, mixer_in.at[0]),
+        (queries_narrow_hbm, mixer_in.at[1]),
+        (out_wide_hbm, outs_in.at[0]),
+        (out_narrow_hbm, outs_in.at[1]),
+        (residual_hbm, residual),
+        (gate_hbm, gate),
+        (up_hbm, up),
+        (down_hbm, down),
+    )
+    every_load = [
+        pltpu.make_async_copy(src, dst, load_sem.at[n]) for n, (src, dst) in enumerate(sources)
     ]
-    for load in loads:
+    for load in every_load:
         load.start()
+    loads = every_load[9:]
+    queries, queries_narrow = mixer_in.at[0], mixer_in.at[1]
+    keys, keys_narrow = mixer_in.at[2], mixer_in.at[3]
+    values, values_narrow = mixer_in.at[4], mixer_in.at[5]
+    out_wide, out_narrow = outs_in.at[0], outs_in.at[1]
 
     barrier = pltpu.get_barrier_semaphore()
     pl.semaphore_signal(barrier, inc=1, device_id={"tp": partner}, device_id_type=MESH)
@@ -129,6 +158,61 @@
         pl.semaphore_signal(barrier, inc=1, device_id={"sp": peer(step)}, device_id_type=MESH)
 
     length = queries.shape[0]
+    rows_dev = residual.shape[0]
+    fine_rows = fine.shape[2]
+    coarse_rows = length // fine_rows
+    at_coarse = pl.multiple_of(place * coarse_rows, coarse_rows)
+    for narrow in range(2):
+        cosine_fine, sine_fine = fine[narrow, 0], fine[narrow, 1]
+        cosine_coarse = coarse[narrow, 0, pl.ds(at_coarse, coarse_rows), :]
+        sine_coarse = coarse[narrow, 1, pl.ds(at_coarse, coarse_rows), :]
+        for at in range(coarse_rows):
+            cosine, sine_part = cosine_coarse[at : at + 1], sine_coarse[at : at + 1]
+            span = slice(at * fine_rows, (at + 1) * fine_rows)
+            turns[narrow, 0, span] = cosine * cosine_fine - sine_part * sine_fine
+            turns[narrow, 1, span] = sine_part * cosine_fine + cosine * sine_fine
+
+    def pieces_of(value):
+        high = value.astype(jnp.bfloat16)
+        rest = value - high.astype(jnp.float32)
+        middle = rest.astype(jnp.bfloat16)
+        low = (rest - middle.astype(jnp.float32)).astype(jnp.bfloat16)
+        return high, middle, low
+
+    row_at = lax.broadcasted_iota(jnp.int32, (128, 128), 0)
+    lane_at = lax.broadcasted_iota(jnp.int32, (128, 128), 1)
+    up_to = (row_at <= lane_at).astype(jnp.bfloat16)
+    heads_wide, heads_narrow = decay_wide.shape[0], decay_narrow.shape[0]
+    decays[...] = jnp.zeros_like(decays)
+    decays[0:heads_wide, :] = decay_wide[...]
+    decays[heads_wide : heads_wide + heads_narrow, :] = decay_narrow[...]
+    running = jnp.zeros((8, 1), jnp.float32)
+    for at in range(0, length, 128):
+        within = running
+        for piece in pieces_of(decays[:, at : at + 128]):
+            within = within + jnp.dot(piece, up_to, preferred_element_type=jnp.float32)
+        log_rows[:, at : at + 128] = within
+        log_columns[at : at + 128, :] = within.T
+        running = within[:, 127:128]
+
+    named = lax.broadcasted_iota(jnp.int32, (slot_rows.shape[0], rows_dev), 0)
+    hits = (routes[0:1, :] == named) | (routes[1:2, :] == named)
+    earlier = lax.broadcasted_iota(jnp.int32, (rows_dev, rows_dev), 0) < lax.broadcasted_iota(
+        jnp.int32, (rows_dev, rows_dev), 1
+    )
+    rank = jnp.dot(
+        hits.astype(jnp.bfloat16),
+        earlier.astype(jnp.bfloat16),
+        preferred_element_type=jnp.float32,
+    )
+    slot_rows[...] = jnp.where(hits, rank, -1.0)
+    slot_columns[...] = slot_rows[...].T
+    weight_columns[...] = (
+        jnp.where(routes[0:1, :] == named, weights[0:1, :], 0.0)
+        + jnp.where(routes[1:2, :] == named, weights[1:2, :], 0.0)
+    ).T
+    for load in every_load[:6]:
+        load.wait()
     lane = lax.broadcasted_iota(jnp.int32, (1, 128), 1)
     first = lane < HEAD_NARROW
     rows_128 = lax.broadcasted_iota(jnp.int32, (128, 128), 0)
@@ -285,8 +369,9 @@
         for n in range(2)
     ]
     to_across = remote(cross, cross_in, a_send.at[2], a_recv.at[2], tp=across)
+    for load in every_load[6:9]:
+        load.wait()
     for n, target in enumerate(targets):
-        rows_dev = residual.shape[0]
         picked = mixed[pl.ds(pl.multiple_of(target * rows_dev, rows_dev), rows_dev), :]
         part[n] = (
             jnp.dot(picked[:, :256], out_wide[...], preferred_element_type=jnp.float32)
@@ -312,10 +397,11 @@
     scale_row = lax.rsqrt(jnp.mean(total * total, axis=-1, keepdims=True) + norm_eps)
     normed = (total * scale_row * gain[...]).astype(jnp.bfloat16)
 
+    slot_at = lax.broadcasted_iota(jnp.int32, (capacity, rows_dev), 0).astype(jnp.float32)
+
     def slots(expert):
-        return jnp.dot(scatter[expert], normed, preferred_element_type=jnp.float32).astype(
-            jnp.bfloat16
-        )
+        scatter = (slot_rows[pl.ds(expert, 1), :] == slot_at).astype(jnp.bfloat16)
+        return jnp.dot(scatter, normed, preferred_element_type=jnp.float32).astype(jnp.bfloat16)
 
     def dispatch(expert):
         return remote(
@@ -476,16 +562,27 @@
         waiting = step
     finish_across(peer(waiting))
 
+    slot_lane = lax.broadcasted_iota(jnp.int32, (rows_dev, capacity), 1).astype(jnp.float32)
+    name_lane = lax.broadcasted_iota(jnp.int32, slot_columns.shape, 1)
+
+    def column_of(table, expert):
+        kept = jnp.where(name_lane == expert, table[...], 0.0)
+        return jnp.sum(kept, axis=1, keepdims=True)
+
+    def add_expert(expert):
+        pick = (column_of(slot_columns, expert) == slot_lane).astype(jnp.bfloat16)
+        hidden_state[...] += column_of(weight_columns, expert) * jnp.dot(
+            pick, returned[expert], preferred_element_type=jnp.float32
+        )
+
+    add_expert(place)
+
     @pl.loop(1, experts)
     def _(step):
         came_back(peer(step)).wait_recv()
-
-    every = returned[...].reshape(experts * capacity, model_width)
+        add_expert(peer(step))
+
     total = hidden_state[...]
-    for k in range(TOP_K):
-        total = total + weights[:, k : k + 1] * jnp.dot(
-            pick[k], every, preferred_element_type=jnp.float32
-        )
     output[...] = total.astype(output.dtype)
 
     @pl.loop(place + 1, experts)
@@ -512,32 +609,33 @@
             give_back(source).wait_send()
 
 
-def layer(mixer_inputs, outs, residual, norm_gain, routes, route_weights, gate, up, down):
+FINE_ROWS = 32
+
+
+def rotary_tables(steps):
+    grids = []
+    for at in (np.arange(0, steps, FINE_ROWS), np.arange(FINE_ROWS)):
+        grid = []
+        for width in (HEAD_WIDE, HEAD_NARROW):
+            half_width = width // 2
+            inverse = np.float32(rotary_base) ** (
+                -np.arange(half_width, dtype=np.float32) / np.float32(half_width)
+            )
+            angles = at[:, None] * np.tile(inverse.astype(np.float64), 128 // half_width)
+            grid.append(np.stack([np.cos(angles), np.sin(angles)]))
+        grids.append(np.stack(grid).astype(np.float32))
+    return grids
+
+
+def layer(mixer_inputs, decays, outs, residual, norm_gain, routes, route_weights, gate, up, down):
     experts = lax.axis_size("sp")
     rows_dev, model_width = residual.shape
     length = mixer_inputs[0].shape[0]
     ff = gate.shape[1]
     limit = max(TOP_K, 3 * rows_dev * TOP_K // (2 * experts))
     capacity = -(-limit // 16) * 16
-    names = jnp.arange(experts, dtype=jnp.int32)
-    chosen = routes[:, :, None] == names[None, None, :]
-    hits = jnp.any(chosen, axis=1)
-    order = jnp.arange(rows_dev, dtype=jnp.int32)
-    before = (order[:, None] > order[None, :]).astype(jnp.bfloat16)
-    rank = jnp.dot(before, hits.astype(jnp.bfloat16), preferred_element_type=jnp.float32).astype(
-        jnp.int32
-    )
-    slot = jnp.arange(capacity, dtype=jnp.int32)
-    at_slot = rank[:, :, None] == slot[None, None, :]
-    pick = (
-        (chosen[:, :, :, None] & at_slot[:, None])
-        .astype(jnp.bfloat16)
-        .transpose(1, 0, 2, 3)
-        .reshape(TOP_K, rows_dev, experts * capacity)
-    )
-    scatter = ((hits.T[:, None, :]) & (rank.T[:, None, :] == slot[None, :, None])).astype(
-        jnp.bfloat16
-    )
+    named = -(-experts // 8) * 8
+    coarse, fine = rotary_tables(experts * length)
     bf16 = jnp.bfloat16
     block = (capacity, model_width)
     dma = pltpu.SemaphoreType.DMA
@@ -546,12 +644,22 @@
     return pl.pallas_call(
         functools.partial(tail_kernel, experts, capacity),
         out_shape=jax.ShapeDtypeStruct((rows_dev, model_width), bf16),
-        in_specs=[vmem] * 16 + [anywhere] * 3,
+        in_specs=[anywhere] * 12 + [vmem] * 7,
         out_specs=vmem,
         scratch_shapes=[
+            pltpu.VMEM((6, *mixer_inputs[0].shape), bf16),
+            pltpu.VMEM((2, *outs[0].shape), bf16),
+            pltpu.VMEM((rows_dev, model_width), bf16),
             pltpu.VMEM((model_width, ff), bf16),
             pltpu.VMEM((model_width, ff), bf16),
             pltpu.VMEM((ff, model_width), bf16),
+            pltpu.VMEM((8, length), jnp.float32),
+            pltpu.VMEM((8, length), jnp.float32),
+            pltpu.VMEM((length, 8), jnp.float32),
+            pltpu.VMEM((2, 2, length, 128), jnp.float32),
+            pltpu.VMEM((named, rows_dev), jnp.float32),
+            pltpu.VMEM((rows_dev, named), jnp.float32),
+            pltpu.VMEM((rows_dev, named), jnp.float32),
             pltpu.VMEM((4, rows_dev, model_width), bf16),
             pltpu.VMEM((2, rows_dev, model_width), bf16),
             pltpu.VMEM((rows_dev, model_width), bf16),
@@ -572,7 +680,7 @@
             pltpu.VMEM((8, 128), jnp.float32),
             pltpu.VMEM((experts, 3, 128, 128), bf16),
             pltpu.VMEM((experts, 8, 128), jnp.float32),
-            dma((3,)),
+            dma((12,)),
             dma((experts,)),
             dma((experts,)),
             dma((experts,)),
@@ -599,13 +707,15 @@
         *mixer_inputs,
         *outs,
         residual,
-        norm_gain.reshape(1, model_width),
-        scatter,
-        pick,
-        route_weights,
         gate,
         up,
         down,
+        *decays,
+        coarse,
+        fine,
+        norm_gain.reshape(1, model_width),
+        routes.T,
+        route_weights.T,
     )
 
 
@@ -628,17 +738,6 @@
     expert_up,
     expert_down,
 ):
-    length = query_wide.shape[0]
-    positions = (lax.axis_index("sp") * length + jnp.arange(length, dtype=jnp.int32)).astype(
-        jnp.float32
-    )
-    tables = []
-    for width in (HEAD_WIDE, HEAD_NARROW):
-        half_width = width // 2
-        inverse = rotary_base ** (-jnp.arange(half_width, dtype=jnp.float32) / half_width)
-        angles = positions[:, None] * jnp.tile(inverse, 128 // half_width)[None, :]
-        tables.append(jnp.stack([jnp.cos(angles), jnp.sin(angles)]))
-    log_columns = jnp.cumsum(jnp.concatenate([decay_wide, decay_narrow], axis=1), axis=0)
     return layer(
         (
             query_wide,
@@ -647,10 +746,8 @@
             key_narrow,
             value_wide,
             value_narrow,
-            log_columns,
-            log_columns.T,
-            jnp.stack(tables),
         ),
+        (decay_wide.T, decay_narrow.T),
         (out_wide, out_narrow),
         residual,
         norm_gain,

time: 134 us -> 123 us (0.918)
  other arithmetic: 6.56 us -> 0 us
  local copies, waits for them, and re-layouts: 4.46 us -> 1.88 us
    another operation x4 -> x0, other arithmetic: 2.99 us -> none
    cos x1 -> x0, other arithmetic: 1.9 us -> none  [body(): tables.append(jnp.stack([jnp.cos(angles), jnp.sin(angles)]))]
    convert_element_type x3 -> x0, other arithmetic: 1.43 us -> none  [the longest x1 0.73 us: layer(): pick = (chosen[:, :, :, None] & at_slot[:, None]).astype(jnp.bfloat16).tr...]
where the time goes in v1:
time: 123 us
  Pallas kernels  121 us (98%)
  local copies, waits for them, and re-layouts  1.88 us (2%)
    pallas_call x1, Pallas kernels, layer(): pl.pallas_call(functools.partial(tail_kernel, experts, capacity), out_sha...  121 us

profile of v1, /device:TPU:0, one launch (start us, length us, event | category | flops | bytes accessed | tf_op | source)
XLA Modules:
  0.0 123.2 jit_solution(13772542881352408710)
XLA Ops:
  0.0 121.3 %shard_map.181 = bf16[128,2048]{1,0:T(8,128)(2,1)} custom-call(bf16[512,256]{1,0:T(8,128)(2,1)} %queries_hbm.1, bf16[512,256]{1,0:T(8,128)(2,1)} %queries_narrow_hbm.1, bf16[512,256]{1,0:T(8,128)(2,1)} %keys_hbm.1, bf16[512,256]{1,0:T(8,128)(2,1)} %keys_narrow_hbm.1, bf16[512,256]{1,0:T(8,128)(2,1)} %values_hbm.1, bf16[512,256]{1,0:T(8,128)(2,1)} %values_narrow_hbm.1, ...), custom_call_target="tpu_custom_call" | custom-call | tf_op jit(solution)/shard_map/pallas_call | solution.py:644
  121.3 1.9 %copy.21 = bf16[128,2048]{1,0:T(8,128)(2,1)} copy(bf16[128,2048]{1,0:T(8,128)(2,1)} %shard_map.181) | data formatting | bytes 1048576

commit v2 on v1

--- a/solution.py
+++ b/solution.py
@@ -71,11 +71,9 @@
     hidden_state,
     send,
     rows,
+    hidden_own,
+    hidden_in,
     result,
-    result_in,
-    half,
-    half_in,
-    summed,
     returned,
     mixed,
     inner,
@@ -97,19 +95,26 @@
     x_recv,
     p_send,
     p_recv,
-    c_send,
-    c_recv,
     h_send,
     h_recv,
     r_send,
     r_recv,
+    w_send,
+    w_recv,
+    y_send,
+    y_recv,
+    d_send,
+    d_recv,
 ):
     place = lax.axis_index("sp")
     mine = lax.axis_index("tp")
     core, side = mine % 2, mine // 2
     partner = side * 2 + (1 - core)
     across = (1 - side) * 2 + core
+    diagonal_peer = (1 - side) * 2 + 1 - core
+    group = lax.axis_index("grp")
     model_width = residual.shape[1]
+    half_model = model_width // 2
 
     def remote(src, dst, send_sem, recv_sem, **where):
         return pltpu.make_async_remote_copy(
@@ -121,8 +126,51 @@
             device_id_type=MESH,
         )
 
+    order = (0, 2, 3, 1)
+    short = experts == len(order)
+
     def peer(step):
+        if short and isinstance(step, int):
+            return place ^ order[step]
         return lax.rem(place + step, experts) if experts & (experts - 1) else place ^ step
+
+    def half_of(which):
+        return pl.ds(pl.multiple_of(which * half_model, half_model), half_model)
+
+    ff = gate.shape[1]
+    pieces = 8
+    piece_rows = ff // pieces
+    far_core = (core + group) % 2
+    far = (1 - side) * 2 + far_core
+
+    def piece_at(n):
+        return pl.ds(n * piece_rows, piece_rows)
+
+    def down_far(n):
+        return remote(
+            down_hbm.at[piece_at(n), half_of(far_core)],
+            down.at[2 + group, piece_at(n)],
+            w_send.at[n],
+            w_recv.at[n],
+            tp=far,
+        )
+
+    def down_group(n, slot):
+        return remote(
+            down.at[slot, piece_at(n)],
+            down.at[slot, piece_at(n)],
+            y_send.at[n],
+            y_recv.at[n],
+            grp=1 - group,
+        )
+
+    def pass_down(n):
+        down_far(n).wait_recv()
+        down_group(n, 2 + group).start()
+
+    down_partner = remote(
+        down_hbm.at[:, half_of(1 - core)], down.at[1], d_send.at[0], d_recv.at[0], tp=partner
+    )
 
     sources = (
         (keys_hbm, mixer_in.at[2]),
@@ -136,7 +184,7 @@
         (residual_hbm, residual),
         (gate_hbm, gate),
         (up_hbm, up),
-        (down_hbm, down),
+        (down_hbm.at[:, half_of(core)], down.at[0]),
     )
     every_load = [
         pltpu.make_async_copy(src, dst, load_sem.at[n]) for n, (src, dst) in enumerate(sources)
@@ -150,12 +198,16 @@
     out_wide, out_narrow = outs_in.at[0], outs_in.at[1]
 
     barrier = pltpu.get_barrier_semaphore()
-    pl.semaphore_signal(barrier, inc=1, device_id={"tp": partner}, device_id_type=MESH)
-    pl.semaphore_signal(barrier, inc=1, device_id={"tp": across}, device_id_type=MESH)
+    for target in (partner, across, diagonal_peer):
+        pl.semaphore_signal(barrier, inc=1, device_id={"tp": target}, device_id_type=MESH)
+    pl.semaphore_signal(barrier, inc=1, device_id={"grp": 1 - group}, device_id_type=MESH)
 
     @pl.loop(1, experts)
     def _(step):
         pl.semaphore_signal(barrier, inc=1, device_id={"sp": peer(step)}, device_id_type=MESH)
+        pl.semaphore_signal(
+            barrier, inc=1, device_id={"sp": peer(step), "tp": partner}, device_id_type=MESH
+        )
 
     length = queries.shape[0]
     rows_dev = residual.shape[0]
@@ -171,6 +223,12 @@
             span = slice(at * fine_rows, (at + 1) * fine_rows)
             turns[narrow, 0, span] = cosine * cosine_fine - sine_part * sine_fine
             turns[narrow, 1, span] = sine_part * cosine_fine + cosine * sine_fine
+
+    pl.semaphore_wait(barrier, 2 * experts + 2)
+    early = pieces - 4
+    for n in range(early):
+        down_far(n).start()
+    down_partner.start()
 
     def pieces_of(value):
         high = value.astype(jnp.bfloat16)
@@ -194,6 +252,95 @@
         log_rows[:, at : at + 128] = within
         log_columns[at : at + 128, :] = within.T
         running = within[:, 127:128]
+
+    for load in every_load[:4]:
+        load.wait()
+    lane = lax.broadcasted_iota(jnp.int32, (1, 128), 1)
+    first = lane < HEAD_NARROW
+    rows_128 = lax.broadcasted_iota(jnp.int32, (128, 128), 0)
+    lanes_128 = lax.broadcasted_iota(jnp.int32, (128, 128), 1)
+    diagonal = (rows_128 < HEAD_NARROW) == (lanes_128 < HEAD_NARROW)
+    flips = []
+    for width in (HEAD_WIDE, HEAD_NARROW):
+        half_width = width // 2
+        upper = lanes_128 % width >= half_width
+        origin = jnp.where(upper, lanes_128 - half_width, lanes_128 + half_width)
+        flips.append(
+            jnp.where(rows_128 == origin, jnp.where(upper, 1.0, -1.0), 0.0).astype(jnp.bfloat16)
+        )
+
+    def unit_of(wide_ref, narrow_ref, unit):
+        ref = narrow_ref if unit >= 2 else wide_ref
+        return ref[:, unit % 2 * 128 : unit % 2 * 128 + 128]
+
+    def per_lane(unit, table):
+        if unit < 2:
+            return table(unit)
+        return jnp.where(first, table(2 * unit - 2), table(2 * unit - 1))
+
+    def heads_of(unit):
+        if unit < 2:
+            return ((unit, None),)
+        return ((2 * unit - 2, first), (2 * unit - 1, ~first))
+
+    def masked(value, keep):
+        return value if keep is None else jnp.where(keep, value, jnp.zeros_like(value))
+
+    def swapped(value):
+        return pltpu.roll(value, HEAD_NARROW, 1)
+
+    def rotated(refs, unit):
+        narrow = unit // 2
+        value = unit_of(*refs, unit)
+        flipped = jnp.dot(value, flips[narrow], preferred_element_type=jnp.float32)
+        return value.astype(jnp.float32) * turns[narrow, 0] + flipped * turns[narrow, 1]
+
+    packed = []
+    for unit in range(4):
+        narrow = unit // 2
+        width = (HEAD_WIDE, HEAD_NARROW)[narrow]
+        value = rotated((keys, keys_narrow), unit)
+        turned[1, unit] = (value * width ** (-0.5)).astype(jnp.bfloat16)
+        gap = per_lane(
+            unit,
+            lambda head: log_columns[length - 1 : length, head : head + 1]
+            - log_columns[:, head : head + 1],
+        )
+        weighted = (turned[1, unit].astype(jnp.float32) * jnp.exp(gap)).astype(jnp.bfloat16)
+        state = lax.dot_general(
+            weighted,
+            unit_of(values, values_narrow, unit),
+            (((0,), (0,)), ((), ())),
+            preferred_element_type=jnp.float32,
+        )
+        last = log_columns[length - 1 : length, :]
+        total_row = per_lane(
+            unit, lambda head: jnp.broadcast_to(last[:, head : head + 1], (1, 128))
+        )
+        if unit == 3:
+            state, total_row = swapped(state), swapped(total_row)
+        packed.append(state)
+        local_total[unit : unit + 1, :] = total_row
+    for unit in range(4, 8):
+        local_total[unit : unit + 1, :] = jnp.zeros((1, 128), jnp.float32)
+    local_state[0] = packed[0].astype(jnp.bfloat16)
+    local_state[1] = packed[1].astype(jnp.bfloat16)
+    local_state[2] = jnp.where(diagonal, packed[2], packed[3]).astype(jnp.bfloat16)
+
+    def send_state(source, target):
+        return remote(
+            local_state, states.at[source], s_send.at[target], s_recv.at[source], sp=target
+        )
+
+    def send_total(source, target):
+        return remote(
+            local_total, totals.at[source], t_send.at[target], t_recv.at[source], sp=target
+        )
+
+    @pl.loop(place + 1, experts)
+    def _(target):
+        send_state(place, target).start()
+        send_total(place, target).start()
 
     named = lax.broadcasted_iota(jnp.int32, (slot_rows.shape[0], rows_dev), 0)
     hits = (routes[0:1, :] == named) | (routes[1:2, :] == named)
@@ -211,96 +358,10 @@
         jnp.where(routes[0:1, :] == named, weights[0:1, :], 0.0)
         + jnp.where(routes[1:2, :] == named, weights[1:2, :], 0.0)
     ).T
-    for load in every_load[:6]:
+    for load in every_load[4:6]:
         load.wait()
-    lane = lax.broadcasted_iota(jnp.int32, (1, 128), 1)
-    first = lane < HEAD_NARROW
-    rows_128 = lax.broadcasted_iota(jnp.int32, (128, 128), 0)
-    lanes_128 = lax.broadcasted_iota(jnp.int32, (128, 128), 1)
-    diagonal = (rows_128 < HEAD_NARROW) == (lanes_128 < HEAD_NARROW)
-    flips = []
-    for width in (HEAD_WIDE, HEAD_NARROW):
-        half_width = width // 2
-        upper = lanes_128 % width >= half_width
-        origin = jnp.where(upper, lanes_128 - half_width, lanes_128 + half_width)
-        flips.append(
-            jnp.where(rows_128 == origin, jnp.where(upper, 1.0, -1.0), 0.0).astype(jnp.bfloat16)
-        )
-
-    def unit_of(wide_ref, narrow_ref, unit):
-        ref = narrow_ref if unit >= 2 else wide_ref
-        return ref[:, unit % 2 * 128 : unit % 2 * 128 + 128]
-
-    def per_lane(unit, table):
-        if unit < 2:
-            return table(unit)
-        return jnp.where(first, table(2 * unit - 2), table(2 * unit - 1))
-
-    def heads_of(unit):
-        if unit < 2:
-            return ((unit, None),)
-        return ((2 * unit - 2, first), (2 * unit - 1, ~first))
-
-    def masked(value, keep):
-        return value if keep is None else jnp.where(keep, value, jnp.zeros_like(value))
-
-    def swapped(value):
-        return pltpu.roll(value, HEAD_NARROW, 1)
-
-    packed = []
     for unit in range(4):
-        narrow = unit // 2
-        cosine, sine_part = turns[narrow, 0], turns[narrow, 1]
-        width = (HEAD_WIDE, HEAD_NARROW)[narrow]
-        for n, refs in enumerate(((queries, queries_narrow), (keys, keys_narrow))):
-            value = unit_of(*refs, unit)
-            flipped = jnp.dot(value, flips[narrow], preferred_element_type=jnp.float32)
-            value = value.astype(jnp.float32) * cosine + flipped * sine_part
-            if n == 1:
-                value = value * width ** (-0.5)
-            turned[n, unit] = value.astype(jnp.bfloat16)
-        gap = per_lane(
-            unit,
-            lambda head: log_columns[length - 1 : length, head : head + 1]
-            - log_columns[:, head : head + 1],
-        )
-        weighted = (turned[1, unit].astype(jnp.float32) * jnp.exp(gap)).astype(jnp.bfloat16)
-        state = lax.dot_general(
-            weighted,
-            unit_of(values, values_narrow, unit),
-            (((0,), (0,)), ((), ())),
-            preferred_element_type=jnp.float32,
-        )
-        last = log_columns[length - 1 : length, :]
-        total_row = per_lane(
-            unit, lambda head: jnp.broadcast_to(last[:, head : head + 1], (1, 128))
-        )
-        if unit == 3:
-            state, total_row = swapped(state), swapped(total_row)
-        packed.append(state)
-        local_total[unit : unit + 1, :] = total_row
-    for unit in range(4, 8):
-        local_total[unit : unit + 1, :] = jnp.zeros((1, 128), jnp.float32)
-    local_state[0] = packed[0].astype(jnp.bfloat16)
-    local_state[1] = packed[1].astype(jnp.bfloat16)
-    local_state[2] = jnp.where(diagonal, packed[2], packed[3]).astype(jnp.bfloat16)
-
-    def send_state(source, target):
-        return remote(
-            local_state, states.at[source], s_send.at[target], s_recv.at[source], sp=target
-        )
-
-    def send_total(source, target):
-        return remote(
-            local_total, totals.at[source], t_send.at[target], t_recv.at[source], sp=target
-        )
-
-    pl.semaphore_wait(barrier, experts + 1)
-
-    @pl.loop(place + 1, experts)
-    def _(target):
-        send_state(place, target).start()
-        send_total(place, target).start()
+        turned[0, unit] = rotated((queries, queries_narrow), unit).astype(jnp.bfloat16)
 
     tile = min(length, 256)
     for unit in range(4):
@@ -337,6 +398,7 @@
             carried[2] * fade_narrow + states[source, 2].astype(jnp.float32),
         )
 
+    pass_down(0)
     nothing = jnp.zeros((128, 128), jnp.float32)
     carried = lax.fori_loop(0, place, join, (nothing, nothing, nothing))
     for unit in range(4):
@@ -363,35 +425,55 @@
             jnp.bfloat16
         )
 
-    targets = (across // 2 * 2 + 1 - core, partner, across, mine)
-    to_partner = [
-        remote(part.at[n], part_in.at[n], a_send.at[n], a_recv.at[n], tp=partner)
-        for n in range(2)
-    ]
-    to_across = remote(cross, cross_in, a_send.at[2], a_recv.at[2], tp=across)
+    columns = 4
+    width = model_width // columns
+
+    def to_partner(n, at):
+        where = (n, slice(None), pl.ds(at * width, width))
+        return remote(
+            part.at[where], part_in.at[where], a_send.at[n, at], a_recv.at[n, at], tp=partner
+        )
+
+    def to_across(at):
+        where = (slice(None), pl.ds(at * width, width))
+        return remote(
+            cross.at[where], cross_in.at[where], a_send.at[2, at], a_recv.at[2, at], tp=across
+        )
+
     for load in every_load[6:9]:
         load.wait()
-    for n, target in enumerate(targets):
+
+    def projected(target, at):
         picked = mixed[pl.ds(pl.multiple_of(target * rows_dev, rows_dev), rows_dev), :]
-        part[n] = (
-            jnp.dot(picked[:, :256], out_wide[...], preferred_element_type=jnp.float32)
-            + jnp.dot(picked[:, 256:], out_narrow[...], preferred_element_type=jnp.float32)
-        ).astype(jnp.bfloat16)
-        if n < 2:
-            to_partner[n].start()
-        if n == 2:
-            to_partner[0].wait_recv()
-            cross[...] = (
-                part[2].astype(jnp.float32) + part_in[0].astype(jnp.float32)
-            ).astype(jnp.bfloat16)
-            to_across.start()
-    to_partner[1].wait_recv()
-    hidden_state[...] = (
-        residual[...].astype(jnp.float32)
-        + part[3].astype(jnp.float32)
-        + part_in[1].astype(jnp.float32)
-    )
-    to_across.wait_recv()
+        span = slice(at * width, (at + 1) * width)
+        return jnp.dot(
+            picked[:, :256], out_wide[:, span], preferred_element_type=jnp.float32
+        ) + jnp.dot(picked[:, 256:], out_narrow[:, span], preferred_element_type=jnp.float32)
+
+    for at in range(columns):
+        span = slice(at * width, (at + 1) * width)
+        part[0, :, span] = projected(diagonal_peer, at).astype(jnp.bfloat16)
+        to_partner(0, at).start()
+    for at in range(columns):
+        span = slice(at * width, (at + 1) * width)
+        value = projected(across, at)
+        to_partner(0, at).wait_recv()
+        cross[:, span] = (value + part_in[0, :, span].astype(jnp.float32)).astype(jnp.bfloat16)
+        to_across(at).start()
+    pass_down(1)
+    for at in range(columns):
+        span = slice(at * width, (at + 1) * width)
+        part[1, :, span] = projected(partner, at).astype(jnp.bfloat16)
+        to_partner(1, at).start()
+    for at in range(columns):
+        span = slice(at * width, (at + 1) * width)
+        value = residual[:, span].astype(jnp.float32) + projected(mine, at)
+        to_partner(1, at).wait_recv()
+        hidden_state[:, span] = value + part_in[1, :, span].astype(jnp.float32)
+    for n in range(2, early):
+        pass_down(n)
+    for at in range(columns):
+        to_across(at).wait_recv()
     total = hidden_state[...] + cross_in[...].astype(jnp.float32)
     hidden_state[...] = total
     scale_row = lax.rsqrt(jnp.mean(total * total, axis=-1, keepdims=True) + norm_eps)
@@ -436,35 +518,58 @@
             tp=partner,
         )
 
-    def swap(source):
+    def hidden_across(source):
+        return remote(
+            hidden_own.at[source, 1 - side],
+            hidden_in.at[source, 1],
+            h_send.at[source, 1],
+            h_recv.at[source, 1],
+            tp=across,
+        )
+
+    def hidden_partner(source):
+        return remote(
+            hidden_own.at[source, side],
+            hidden_in.at[source, 0],
+            h_send.at[source, 0],
+            h_recv.at[source, 0],
+            tp=partner,
+        )
+
+    def hidden_forward(source):
+        return remote(
+            hidden_in.at[source, 1],
+            hidden_in.at[source, 2],
+            h_send.at[source, 2],
+            h_recv.at[source, 2],
+            tp=partner,
+        )
+
+    def give_back(source):
+        return remote(
+            result.at[source, core],
+            returned.at[place, core],
+            r_send.at[source, 0],
+            r_recv.at[place, core],
+            sp=source,
+        )
+
+    def give_partner(source):
         return remote(
             result.at[source, 1 - core],
-            result_in.at[source],
-            c_send.at[source],
-            c_recv.at[source],
+            returned.at[place, core],
+            r_send.at[source, 1],
+            r_recv.at[place, core],
+            sp=source,
             tp=partner,
         )
 
-    def swap_across(source):
-        return remote(
-            half.at[source], half_in.at[source], h_send.at[source], h_recv.at[source], tp=across
-        )
-
-    def give_back(source):
-        return remote(
-            summed.at[source],
-            returned.at[place],
-            r_send.at[source],
-            r_recv.at[place],
-            sp=source,
-        )
-
-    def came_back(expert):
-        return remote(
-            summed.at[expert],
-            returned.at[expert],
-            r_send.at[expert],
-            r_recv.at[expert],
+    def came_back(expert, which):
+        return remote(
+            result.at[expert, 0],
+            returned.at[expert, which],
+            r_send.at[expert, 0],
+            r_recv.at[expert, which],
             sp=expert,
         )
 
@@ -475,92 +580,140 @@
         dispatch(expert).start()
 
     rows[place, mine] = slots(place)
-    forward_across(place).start()
-    forward_partner(place, 0).start()
 
     for load in loads:
         load.wait()
 
-    ff = gate.shape[1]
     ff_step = min(ff, 256)
-    out_step = min(model_width, 512)
-
-    def finish_across(source):
-        swap_across(source).wait_recv()
-        value = (
-            result[source, core, side].astype(jnp.float32)
-            + result_in[source, side].astype(jnp.float32)
-            + half_in[source].astype(jnp.float32)
-        ).astype(jnp.bfloat16)
+    out_step = min(half_model, 512)
+
+    def spread(source):
+        hidden_across(source).wait_recv()
+        hidden_forward(source).start()
+
+    def finish(source):
+        hidden_partner(source).wait_recv()
+        hidden_forward(source).wait_recv()
+        for at in range(0, half_model, out_step):
+            span = slice(at, at + out_step)
+            value = jnp.dot(
+                hidden_own[source, side], down[0, :, span], preferred_element_type=jnp.float32
+            )
+            for n in range(3):
+                value = value + jnp.dot(
+                    hidden_in[source, n], down[n + 1, :, span], preferred_element_type=jnp.float32
+                )
+            value = value.astype(jnp.bfloat16)
+            for n in range(2):
+                result[source, n, :, span] = value[n * capacity : (n + 1) * capacity]
 
         @pl.when(source == place)
         def _():
-            returned[place] = value
+            returned[place, core] = result[place, core]
+            remote(
+                result.at[place, 1 - core],
+                returned.at[place, core],
+                r_send.at[place, 1],
+                r_recv.at[place, core],
+                tp=partner,
+            ).start()
 
         @pl.when(source != place)
         def _():
-            summed[source] = value
             give_back(source).start()
-
-    late = min(2, experts - 1)
-
-    def halve(source):
-        swap(source).wait_recv()
-        half[source] = (
-            result[source, core, 1 - side].astype(jnp.float32)
-            + result_in[source, 1 - side].astype(jnp.float32)
-        ).astype(jnp.bfloat16)
-        swap_across(source).start()
-
-    @pl.loop(0, experts)
-    def _(step):
-        source = peer(step)
-
-        @pl.when(step + 1 < experts)
-        def _():
-            later = peer(step + 1)
-            arrived(later).wait_recv()
-            forward_across(later).start()
-            forward_partner(later, 0).start()
-
+            give_partner(source).start()
+
+    def take(step):
+        later = peer(step)
+        arrived(later).wait_recv()
+        forward_across(later).start()
+        forward_partner(later, 0).start()
+
+    def expand(source):
         forward_across(source).wait_recv()
         forward_partner(source, 1).start()
         forward_partner(source, 0).wait_recv()
         forward_partner(source, 1).wait_recv()
         block = rows[source].reshape(4 * capacity, model_width)
-        hidden = []
         for at in range(0, ff, ff_step):
-            gate_pre = jnp.dot(
-                block, gate[:, at : at + ff_step], preferred_element_type=jnp.float32
-            )
-            up_pre = jnp.dot(block, up[:, at : at + ff_step], preferred_element_type=jnp.float32)
-            hidden.append(activate(gate_pre, up_pre).astype(jnp.bfloat16))
-        hidden = jnp.concatenate(hidden, axis=1)
-        for at in range(0, model_width, out_step):
-            value = jnp.dot(
-                hidden, down[:, at : at + out_step], preferred_element_type=jnp.float32
-            ).astype(jnp.bfloat16)
-            for n in range(4):
-                result[source, n % 2, n // 2, :, at : at + out_step] = value[
-                    n * capacity : (n + 1) * capacity
-                ]
-        swap(source).start()
-
-        @pl.when(step >= late)
-        def _():
-            halve(source)
-
-        @pl.when(step > late)
-        def _():
-            finish_across(peer(step - 1))
-
-    waiting = experts - 1 if experts > late else None
-    for step in range(late - 1, -1, -1):
-        halve(peer(step))
-        if waiting is not None:
-            finish_across(peer(waiting))
-        waiting = step
-    finish_across(peer(waiting))
+            span = slice(at, at + ff_step)
+            gate_pre = jnp.dot(block, gate[:, span], preferred_element_type=jnp.float32)
+            up_pre = jnp.dot(block, up[:, span], preferred_element_type=jnp.float32)
+            value = activate(gate_pre, up_pre).astype(jnp.bfloat16)
+            for n in range(2):
+                hidden_own[source, n, :, span] = value[2 * n * capacity : 2 * (n + 1) * capacity]
+
+    def swap_hidden(source):
+        hidden_across(source).start()
+        hidden_partner(source).start()
+
+    if short:
+        for n in range(early, pieces):
+            down_far(n).start()
+        forward_across(place).start()
+        forward_partner(place, 0).start()
+        take(1)
+        expand(place)
+        take(3)
+        for n in range(early, pieces):
+            pass_down(n)
+        expand(peer(1))
+        swap_hidden(peer(1))
+        take(2)
+        expand(peer(3))
+        swap_hidden(peer(3))
+        down_partner.wait_recv()
+        for n in range(pieces):
+            down_group(n, 3 - group).wait_recv()
+        spread(peer(1))
+        finish(peer(1))
+        expand(peer(2))
+        swap_hidden(peer(2))
+        spread(peer(3))
+        finish(peer(3))
+        spread(peer(2))
+        finish(peer(2))
+        swap_hidden(place)
+        spread(place)
+        finish(place)
+    else:
+        forward_across(place).start()
+        forward_partner(place, 0).start()
+        take(1)
+        for n in range(early, pieces):
+            down_far(n).start()
+        expand(place)
+
+        @pl.loop(1, experts)
+        def _(step):
+            source = peer(step)
+            expand(source)
+            swap_hidden(source)
+
+            @pl.when(step == 1)
+            def _():
+                for n in range(early, pieces):
+                    pass_down(n)
+
+            @pl.when(step + 1 < experts)
+            def _():
+                take(step + 1)
+
+            @pl.when(step + 1 == experts)
+            def _():
+                swap_hidden(place)
+
+            @pl.when(step == 1)
+            def _():
+                down_partner.wait_recv()
+                for n in range(pieces):
+                    down_group(n, 3 - group).wait_recv()
+
+            spread(source)
+            finish(source)
+
+        spread(place)
+        finish(place)
 
     slot_lane = lax.broadcasted_iota(jnp.int32, (rows_dev, capacity), 1).astype(jnp.float32)
     name_lane = lax.broadcasted_iota(jnp.int32, slot_columns.shape, 1)
@@ -571,16 +724,22 @@
 
     def add_expert(expert):
         pick = (column_of(slot_columns, expert) == slot_lane).astype(jnp.bfloat16)
-        hidden_state[...] += column_of(weight_columns, expert) * jnp.dot(
-            pick, returned[expert], preferred_element_type=jnp.float32
-        )
-
+        weight = column_of(weight_columns, expert)
+        for n in range(2):
+            span = slice(n * half_model, (n + 1) * half_model)
+            hidden_state[:, span] += weight * jnp.dot(
+                pick, returned[expert, n], preferred_element_type=jnp.float32
+            )
+
+    came_back(place, 1 - core).wait_recv()
     add_expert(place)
 
     @pl.loop(1, experts)
     def _(step):
-        came_back(peer(step)).wait_recv()
-        add_expert(peer(step))
+        expert = peer(step)
+        came_back(expert, 0).wait_recv()
+        came_back(expert, 1).wait_recv()
+        add_expert(expert)
 
     total = hidden_state[...]
     output[...] = total.astype(output.dtype)
@@ -590,9 +749,14 @@
         send_state(place, target).wait_send()
         send_total(place, target).wait_send()
 
-    to_partner[0].wait_send()
-    to_partner[1].wait_send()
-    to_across.wait_send()
+    for at in range(columns):
+        to_partner(0, at).wait_send()
+        to_partner(1, at).wait_send()
+        to_across(at).wait_send()
+    for n in range(pieces):
+        down_far(n).wait_send()
+        down_group(n, 2 + group).wait_send()
+    down_partner.wait_send()
 
     @pl.loop(0, experts)
     def _(step):
@@ -600,8 +764,10 @@
         forward_across(source).wait_send()
         forward_partner(source, 0).wait_send()
         forward_partner(source, 1).wait_send()
-        swap(source).wait_send()
-        swap_across(source).wait_send()
+        hidden_across(source).wait_send()
+        hidden_partner(source).wait_send()
+        hidden_forward(source).wait_send()
+        give_partner(source).wait_send()
 
         @pl.when(step >= 1)
         def _():
@@ -652,7 +818,7 @@
             pltpu.VMEM((rows_dev, model_width), bf16),
             pltpu.VMEM((model_width, ff), bf16),
             pltpu.VMEM((model_width, ff), bf16),
-            pltpu.VMEM((ff, model_width), bf16),
+            pltpu.VMEM((4, ff, model_width // 2), bf16),
             pltpu.VMEM((8, length), jnp.float32),
             pltpu.VMEM((8, length), jnp.float32),
             pltpu.VMEM((length, 8), jnp.float32),
@@ -667,12 +833,10 @@
             pltpu.VMEM((rows_dev, model_width), jnp.float32),
             pltpu.VMEM((experts, *block), bf16),
             pltpu.VMEM((experts, 4, *block), bf16),
-            pltpu.VMEM((experts, 2, 2, *block), bf16),
-            pltpu.VMEM((experts, 2, *block), bf16),
-            pltpu.VMEM((experts, *block), bf16),
-            pltpu.VMEM((experts, *block), bf16),
-            pltpu.VMEM((experts, *block), bf16),
-            pltpu.VMEM((experts, *block), bf16),
+            pltpu.VMEM((experts, 2, 2 * capacity, ff), bf16),
+            pltpu.VMEM((experts, 3, 2 * capacity, ff), bf16),
+            pltpu.VMEM((experts, 2, capacity, model_width // 2), bf16),
+            pltpu.VMEM((experts, 2, capacity, model_width // 2), bf16),
             pltpu.VMEM((length, 512), bf16),
             pltpu.VMEM((4, length, 128), jnp.float32),
             pltpu.VMEM((2, 4, length, 128), bf16),
@@ -685,20 +849,24 @@
             dma((experts,)),
             dma((experts,)),
             dma((experts,)),
-            dma((3,)),
-            dma((3,)),
+            dma((3, 4)),
+            dma((3, 4)),
             dma((experts,)),
             dma((experts,)),
             dma((experts,)),
             dma((experts,)),
             dma((experts, 2)),
             dma((experts, 2)),
-            dma((experts,)),
-            dma((experts,)),
-            dma((experts,)),
-            dma((experts,)),
-            dma((experts,)),
-            dma((experts,)),
+            dma((experts, 3)),
+            dma((experts, 3)),
+            dma((experts, 2)),
+            dma((experts, 2)),
+            dma((8,)),
+            dma((8,)),
+            dma((8,)),
+            dma((8,)),
+            dma((1,)),
+            dma((1,)),
         ],
         compiler_params=pltpu.CompilerParams(
             collective_id=1, has_side_effects=True, vmem_limit_bytes=60 * 1024 * 1024

time: 123 us -> 121 us (0.984)
  Pallas kernels: 121 us -> 118 us
    pallas_call x1, Pallas kernels: 121 us -> 118 us  [layer(): pl.pallas_call(functools.partial(tail_kernel, experts, capacity), out_sha...]
where the time goes in v2:
time: 121 us; the launch traced here: 120 us
  Pallas kernels  118 us (98%)
  local copies, waits for them, and re-layouts  1.88 us (2%)
    pallas_call x1, Pallas kernels, layer(): pl.pallas_call(functools.partial(tail_kernel, experts, capacity), out_sha...  118 us

profile of v2, /device:TPU:0, one launch (start us, length us, event | category | flops | bytes accessed | tf_op | source)
XLA Modules:
  0.0 120.3 jit_solution(3818814290484804898)
XLA Ops:
  0.0 118.4 %shard_map.181 = bf16[128,2048]{1,0:T(8,128)(2,1)} custom-call(bf16[512,256]{1,0:T(8,128)(2,1)} %queries_hbm.1, bf16[512,256]{1,0:T(8,128)(2,1)} %queries_narrow_hbm.1, bf16[512,256]{1,0:T(8,128)(2,1)} %keys_hbm.1, bf16[512,256]{1,0:T(8,128)(2,1)} %keys_narrow_hbm.1, bf16[512,256]{1,0:T(8,128)(2,1)} %values_hbm.1, bf16[512,256]{1,0:T(8,128)(2,1)} %values_narrow_hbm.1, ...), custom_call_target="tpu_custom_call" | custom-call | tf_op jit(solution)/shard_map/pallas_call | solution.py:810
  118.5 1.9 %copy.21 = bf16[128,2048]{1,0:T(8,128)(2,1)} copy(bf16[128,2048]{1,0:T(8,128)(2,1)} %shard_map.181) | data formatting | bytes 1048576

commit v3 on v2

--- a/solution.py
+++ b/solution.py
@@ -126,7 +126,7 @@
             device_id_type=MESH,
         )
 
-    order = (0, 2, 3, 1)
+    order = (0, 1, 2, 3)
     short = experts == len(order)
 
     def peer(step):
@@ -209,6 +209,12 @@
             barrier, inc=1, device_id={"sp": peer(step), "tp": partner}, device_id_type=MESH
         )
 
+    pl.semaphore_wait(barrier, 2 * experts + 2)
+    early = pieces - 3
+    for n in range(early):
+        down_far(n).start()
+    down_partner.start()
+
     length = queries.shape[0]
     rows_dev = residual.shape[0]
     fine_rows = fine.shape[2]
@@ -223,12 +229,6 @@
             span = slice(at * fine_rows, (at + 1) * fine_rows)
             turns[narrow, 0, span] = cosine * cosine_fine - sine_part * sine_fine
             turns[narrow, 1, span] = sine_part * cosine_fine + cosine * sine_fine
-
-    pl.semaphore_wait(barrier, 2 * experts + 2)
-    early = pieces - 4
-    for n in range(early):
-        down_far(n).start()
-    down_partner.start()
 
     def pieces_of(value):
         high = value.astype(jnp.bfloat16)
@@ -485,38 +485,60 @@
         scatter = (slot_rows[pl.ds(expert, 1), :] == slot_at).astype(jnp.bfloat16)
         return jnp.dot(scatter, normed, preferred_element_type=jnp.float32).astype(jnp.bfloat16)
 
-    def dispatch(expert):
-        return remote(
-            send.at[expert],
-            rows.at[place, mine],
-            z_send.at[expert],
-            z_recv.at[place],
+    shares = 2 if capacity % 32 == 0 else 1
+    share = capacity // shares
+
+    def share_at(n):
+        return pl.ds(n * share, share)
+
+    def dispatch(expert, n):
+        return remote(
+            send.at[expert, share_at(n)],
+            rows.at[place, mine, share_at(n)],
+            z_send.at[expert, n],
+            z_recv.at[place, n],
             sp=expert,
         )
 
-    def arrived(source):
-        return remote(
-            send.at[source], rows.at[source, mine], z_send.at[source], z_recv.at[source], sp=source
-        )
-
-    def forward_across(source):
-        return remote(
-            rows.at[source, mine],
-            rows.at[source, mine],
-            x_send.at[source],
-            x_recv.at[source],
+    def arrived(source, n):
+        return remote(
+            send.at[source, share_at(n)],
+            rows.at[source, mine, share_at(n)],
+            z_send.at[source, n],
+            z_recv.at[source, n],
+            sp=source,
+        )
+
+    def forward_across(source, n):
+        return remote(
+            rows.at[source, mine, share_at(n)],
+            rows.at[source, mine, share_at(n)],
+            x_send.at[source, n],
+            x_recv.at[source, n],
             tp=across,
         )
 
     def forward_partner(source, n):
-        block = (mine, across)[n]
-        return remote(
-            rows.at[source, block],
-            rows.at[source, block],
+        return remote(
+            rows.at[source, mine, share_at(n)],
+            rows.at[source, mine, share_at(n)],
             p_send.at[source, n],
             p_recv.at[source, n],
             tp=partner,
         )
+
+    def pass_across(source, n):
+        return remote(
+            rows.at[source, across, share_at(n)],
+            rows.at[source, across, share_at(n)],
+            p_send.at[source, shares + n],
+            p_recv.at[source, shares + n],
+            tp=partner,
+        )
+
+    def forward(source, n):
+        forward_across(source, n).start()
+        forward_partner(source, n).start()
 
     def hidden_across(source):
         return remote(
@@ -577,7 +599,8 @@
     def _(step):
         expert = peer(step)
         send[expert] = slots(expert)
-        dispatch(expert).start()
+        for n in range(shares):
+            dispatch(expert, n).start()
 
     rows[place, mine] = slots(place)
 
@@ -625,15 +648,17 @@
 
     def take(step):
         later = peer(step)
-        arrived(later).wait_recv()
-        forward_across(later).start()
-        forward_partner(later, 0).start()
+        for n in range(shares):
+            arrived(later, n).wait_recv()
+            forward(later, n)
 
     def expand(source):
-        forward_across(source).wait_recv()
-        forward_partner(source, 1).start()
-        forward_partner(source, 0).wait_recv()
-        forward_partner(source, 1).wait_recv()
+        for n in range(shares):
+            forward_across(source, n).wait_recv()
+            pass_across(source, n).start()
+        for n in range(shares):
+            forward_partner(source, n).wait_recv()
+            pass_across(source, n).wait_recv()
         block = rows[source].reshape(4 * capacity, model_width)
         for at in range(0, ff, ff_step):
             span = slice(at, at + ff_step)
@@ -650,35 +675,35 @@
     if short:
         for n in range(early, pieces):
             down_far(n).start()
-        forward_across(place).start()
-        forward_partner(place, 0).start()
         take(1)
-        expand(place)
-        take(3)
+        take(2)
+        expand(peer(1))
         for n in range(early, pieces):
             pass_down(n)
-        expand(peer(1))
         swap_hidden(peer(1))
-        take(2)
-        expand(peer(3))
-        swap_hidden(peer(3))
+        expand(peer(2))
+        swap_hidden(peer(2))
+        take(3)
+        for n in range(shares):
+            forward(place, n)
         down_partner.wait_recv()
         for n in range(pieces):
             down_group(n, 3 - group).wait_recv()
+        spread(peer(2))
+        finish(peer(2))
         spread(peer(1))
         finish(peer(1))
-        expand(peer(2))
-        swap_hidden(peer(2))
+        expand(peer(3))
+        swap_hidden(peer(3))
+        expand(place)
+        swap_hidden(place)
         spread(peer(3))
         finish(peer(3))
-        spread(peer(2))
-        finish(peer(2))
-        swap_hidden(place)
         spread(place)
         finish(place)
     else:
-        forward_across(place).start()
-        forward_partner(place, 0).start()
+        for n in range(shares):
+            forward(place, n)
         take(1)
         for n in range(early, pieces):
             down_far(n).start()
@@ -761,9 +786,10 @@
     @pl.loop(0, experts)
     def _(step):
         source = peer(step)
-        forward_across(source).wait_send()
-        forward_partner(source, 0).wait_send()
-        forward_partner(source, 1).wait_send()
+        for n in range(shares):
+            forward_across(source, n).wait_send()
+            forward_partner(source, n).wait_send()
+            pass_across(source, n).wait_send()
         hidden_across(source).wait_send()
         hidden_partner(source).wait_send()
         hidden_forward(source).wait_send()
@@ -771,7 +797,8 @@
 
         @pl.when(step >= 1)
         def _():
-            dispatch(source).wait_send()
+            for n in range(shares):
+                dispatch(source, n).wait_send()
             give_back(source).wait_send()
 
 
@@ -851,12 +878,12 @@
             dma((experts,)),
             dma((3, 4)),
             dma((3, 4)),
-            dma((experts,)),
-            dma((experts,)),
-            dma((experts,)),
-            dma((experts,)),
             dma((experts, 2)),
             dma((experts, 2)),
+            dma((experts, 2)),
+            dma((experts, 2)),
+            dma((experts, 4)),
+            dma((experts, 4)),
             dma((experts, 3)),
             dma((experts, 3)),
             dma((experts, 2)),

time: 121 us -> 116 us (0.959)
  Pallas kernels: 118 us -> 113 us
    pallas_call x1, Pallas kernels: 118 us -> 113 us  [layer(): pl.pallas_call(functools.partial(tail_kernel, experts, capacity), out_sha...]
where the time goes in v3:
time: 116 us; the launch traced here: 115 us
  Pallas kernels  113 us (97%)
  local copies, waits for them, and re-layouts  1.88 us (2%)
    pallas_call x1, Pallas kernels, layer(): pl.pallas_call(functools.partial(tail_kernel, experts, capacity), out_sha...  113 us

profile of v3, /device:TPU:0, one launch (start us, length us, event | category | flops | bytes accessed | tf_op | source)
XLA Modules:
  0.0 114.9 jit_solution(9800099477609392039)
XLA Ops:
  0.0 113.0 %shard_map.181 = bf16[128,2048]{1,0:T(8,128)(2,1)} custom-call(bf16[512,256]{1,0:T(8,128)(2,1)} %queries_hbm.1, bf16[512,256]{1,0:T(8,128)(2,1)} %queries_narrow_hbm.1, bf16[512,256]{1,0:T(8,128)(2,1)} %keys_hbm.1, bf16[512,256]{1,0:T(8,128)(2,1)} %keys_narrow_hbm.1, bf16[512,256]{1,0:T(8,128)(2,1)} %values_hbm.1, bf16[512,256]{1,0:T(8,128)(2,1)} %values_narrow_hbm.1, ...), custom_call_target="tpu_custom_call" | custom-call | tf_op jit(solution)/shard_map/pallas_call | solution.py:837
  113.0 1.9 %copy.21 = bf16[128,2048]{1,0:T(8,128)(2,1)} copy(bf16[128,2048]{1,0:T(8,128)(2,1)} %shard_map.181) | data formatting | bytes 1048576

commit v4 on v3

--- a/solution.py
+++ b/solution.py
@@ -684,8 +684,7 @@
         expand(peer(2))
         swap_hidden(peer(2))
         take(3)
-        for n in range(shares):
-            forward(place, n)
+        forward(place, 0)
         down_partner.wait_recv()
         for n in range(pieces):
             down_group(n, 3 - group).wait_recv()
@@ -695,6 +694,8 @@
         finish(peer(1))
         expand(peer(3))
         swap_hidden(peer(3))
+        for n in range(1, shares):
+            forward(place, n)
         expand(place)
         swap_hidden(place)
         spread(peer(3))

time: 116 us -> 120 us (1.034)
  Pallas kernels: 113 us -> 117 us
    pallas_call x1, Pallas kernels: 113 us -> 117 us  [layer(): pl.pallas_call(functools.partial(tail_kernel, experts, capacity), out_sha...]
where the time goes in v4:
time: 120 us; the launch traced here: 119 us
  Pallas kernels  117 us (98%)
  local copies, waits for them, and re-layouts  1.88 us (2%)
    pallas_call x1, Pallas kernels, layer(): pl.pallas_call(functools.partial(tail_kernel, experts, capacity), out_sha...  117 us

profile of v4, /device:TPU:0, one launch (start us, length us, event | category | flops | bytes accessed | tf_op | source)
XLA Modules:
  0.0 119.4 jit_solution(18373994945041119065)
XLA Ops:
  0.0 117.5 %shard_map.181 = bf16[128,2048]{1,0:T(8,128)(2,1)} custom-call(bf16[512,256]{1,0:T(8,128)(2,1)} %queries_hbm.1, bf16[512,256]{1,0:T(8,128)(2,1)} %queries_narrow_hbm.1, bf16[512,256]{1,0:T(8,128)(2,1)} %keys_hbm.1, bf16[512,256]{1,0:T(8,128)(2,1)} %keys_narrow_hbm.1, bf16[512,256]{1,0:T(8,128)(2,1)} %values_hbm.1, bf16[512,256]{1,0:T(8,128)(2,1)} %values_narrow_hbm.1, ...), custom_call_target="tpu_custom_call" | custom-call | tf_op jit(solution)/shard_map/pallas_call | solution.py:838
  117.5 1.9 %copy.21 = bf16[128,2048]{1,0:T(8,128)(2,1)} copy(bf16[128,2048]{1,0:T(8,128)(2,1)} %shard_map.181) | data formatting | bytes 1048576
